TPU v7x, 256 devices: a whole 4x4x8 slice. The times are simulated.
256 devices in a mesh: sp: 16 (over y, x), tp: 16 (over z, core).
Axes of the slice: x: 4, y: 4, z: 8, core: 2. Of those that a mesh axis runs over, the one named last changes fastest.
Arguments:
- gate_b: bfloat16 [8192, 1024], P('sp', 'tp'), may hold values from -6 to 6
- gate_c: bfloat16 [8192, 1024], P('sp', 'tp'), may hold values from -6 to 6
- values_in: bfloat16 [8192, 1024], P('sp', 'tp'), may hold values from -6 to 6
- conv_w: bfloat16 [3, 1024], P(None, 'tp'), may hold values from -3.5 to 3.5
- documents: int32 [8192], P('sp'), may hold values from 0 to 8, never falling along the last dimension, each value on 1 to 4096 neighbouring positions
- w_out: bfloat16 [1024, 2048], replicated, may hold values from -0.1875 to 0.1875
- resid: bfloat16 [8192, 2048], P(('sp', 'tp')), may hold values from -6 to 6
- norm_gain: bfloat16 [2048], replicated, may hold values from 0.099609375 to 1.8984375
- route_ids: int32 [8192, 2], P(('sp', 'tp')), may hold values from 0 to 15, all different within a row; in each aligned block of 32 rows (0 to 31, 32 to 63, ...) at most 8 rows name the same one
- route_weight: float32 [8192, 2], P(('sp', 'tp')), may hold values from 0.2 to 1
- w_gate: bfloat16 [16, 2048, 7168], P('sp', None, 'tp'), may hold values from -0.125 to 0.125
- w_up: bfloat16 [16, 2048, 7168], P('sp', None, 'tp'), may hold values from -0.125 to 0.125
- w_down: bfloat16 [16, 7168, 2048], P('sp', 'tp'), may hold values from -0.0625 to 0.0625
Outputs:
- layer_out: bfloat16 [8192, 2048], P(('sp', 'tp'))
Inputs may be any that keep to these rules, and one draw needn't show every extreme that they name: `route_ids`: each token names two different experts; in the rows of one device no expert is named by more than 8 rows, a bound that some block reaches. `documents`: document numbers never fall along the positions; a document has at most 8192 // 2 positions.
All inputs are finite; a program needn't handle non-finite values.
Results may differ from a plain program's by a relative error of at most 0.018.
Values may be sent and summed in bfloat16 or wider, within the bound.
No kernel may reach another device: no remote copies, remote signals or barrier semaphores. Data moves between devices by JAX's collectives and lax.ppermute only.
A program may use at most 128 MiB of HBM per device.

v0:
```python
import jax
import jax.numpy as jnp
from jax import lax
from jax.sharding import PartitionSpec as P


def passed_along(block, axis, distance):
    devices = range(lax.axis_size(axis))
    route = [(i - distance, i) for i in devices if i - distance in devices]
    return lax.ppermute(block, axis, route)


def local(
    gate_b,
    gate_c,
    values_in,
    conv_w,
    documents,
    w_out,
    resid,
    norm_gain,
    route_ids,
    route_weight,
    w_gate,
    w_up,
    w_down,
):
    seq_rows = gate_b.shape[0]
    local_rows = resid.shape[0]
    model_width = resid.shape[1]
    last_rows = jnp.stack([gate_c[seq_rows - 2 :], values_in[seq_rows - 2 :]])
    before, before_docs = passed_along((last_rows, documents[seq_rows - 2 :]), "sp", 1)
    products = jnp.concatenate(
        [
            before[0].astype(jnp.float32) * before[1].astype(jnp.float32),
            gate_c.astype(jnp.float32) * values_in.astype(jnp.float32),
        ],
        axis=0,
    )
    docs_all = jnp.concatenate([before_docs, documents], axis=0)
    kernel_taps = conv_w.astype(jnp.float32)
    near_mask = (docs_all[1:-1] == documents).astype(jnp.float32)[:, None]
    far_mask = (docs_all[:-2] == documents).astype(jnp.float32)[:, None]
    convolved = (
        kernel_taps[2] * products[2:]
        + kernel_taps[1] * products[1:-1] * near_mask
        + kernel_taps[0] * products[:-2] * far_mask
    )
    mixed_rows = (gate_b.astype(jnp.float32) * convolved).astype(jnp.bfloat16)
    token_rows = lax.all_to_all(mixed_rows, "tp", split_axis=0, concat_axis=1, tiled=True)
    projected = jnp.dot(token_rows, w_out, preferred_element_type=jnp.float32)
    hidden_state = (resid.astype(jnp.float32) + projected).astype(jnp.bfloat16)
    state_wide = hidden_state.astype(jnp.float32)
    normed = (
        state_wide
        * lax.rsqrt(jnp.mean(state_wide * state_wide, axis=-1, keepdims=True) + 1e-06)
        * norm_gain.astype(jnp.float32)
    ).astype(jnp.bfloat16)
    experts = lax.axis_size("sp") * w_gate.shape[0]
    capacity = 4 * local_rows // experts
    flat_ids = route_ids.reshape(-1)
    one_hot = (flat_ids[:, None] == jnp.arange(experts, dtype=jnp.int32)[None, :]).astype(jnp.int32)
    rank_in = jnp.sum((jnp.cumsum(one_hot, axis=0) - one_hot) * one_hot, axis=1)
    slot_index = flat_ids * capacity + rank_in
    placement = (
        slot_index[:, None] == jnp.arange(experts * capacity, dtype=jnp.int32)[None, :]
    ).astype(jnp.bfloat16)
    repeated = jnp.repeat(normed, 2, axis=0)
    dispatch = jnp.einsum(
        "js,jd->sd", placement, repeated, preferred_element_type=jnp.float32
    ).astype(jnp.bfloat16)
    dispatch = dispatch.reshape(experts, capacity, model_width)
    gathered_piece = lax.all_gather(
        lax.all_to_all(dispatch, "sp", split_axis=0, concat_axis=0, tiled=True),
        "tp",
        axis=0,
        tiled=True,
    )
    flat_rows = gathered_piece.reshape(-1, model_width)
    gate_part = jnp.dot(flat_rows, w_gate[0], preferred_element_type=jnp.float32)
    up_part = jnp.dot(flat_rows, w_up[0], preferred_element_type=jnp.float32)
    activated = (jax.nn.silu(gate_part) * up_part).astype(jnp.bfloat16)
    partial_value = jnp.dot(activated, w_down[0], preferred_element_type=jnp.float32)
    partial_value = partial_value.reshape(
        gathered_piece.shape[0], gathered_piece.shape[1], model_width
    )
    summed = lax.psum_scatter(
        partial_value.astype(jnp.bfloat16), "tp", scatter_dimension=0, tiled=True
    )
    returned = lax.all_to_all(summed, "sp", split_axis=0, concat_axis=0, tiled=True)
    picked = jnp.take(
        returned.reshape(experts * capacity, model_width), slot_index, axis=0
    ).reshape(local_rows, 2, model_width)
    combined = jnp.sum(route_weight[:, :, None] * picked.astype(jnp.float32), axis=1)
    return (hidden_state.astype(jnp.float32) + combined).astype(jnp.bfloat16)


def solution(mesh):
    return jax.shard_map(
        local,
        mesh=mesh,
        in_specs=(
            P("sp", "tp"),
            P("sp", "tp"),
            P("sp", "tp"),
            P(None, "tp"),
            P("sp"),
            P(),
            P(("sp", "tp"), None),
            P(),
            P(("sp", "tp"), None),
            P(("sp", "tp"), None),
            P("sp", None, "tp"),
            P("sp", None, "tp"),
            P("sp", "tp", None),
        ),
        out_specs=P(("sp", "tp"), None),
        check_vma=False,
    )
```

profile of v0, /device:TPU:2, one launch (start us, length us, event | category | flops | bytes accessed | tf_op | source)
XLA Modules:
  0.0 234.4 jit_solution(8225996941570353827)
XLA Ops:
  6.5 0.9 slice.43
  7.4 3.4 %collective-permute-start.1 = (s32[2]{0:T(128)S(1)}, s32[2]{0:T(128)S(1)}, u32[]{:S(2)}, u32[]{:S(2)}) collective-permute-start(s32[2]{0:T(128)S(1)} %slice.43), channel_id=1, source_target_pairs={{0,16},{16,32},{32,48},{48,64},{64,80},{80,96},{96,112},{112,128},... | collective-permute-start | bytes 32 | tf_op jit(solution)/shard_map/ppermute | solution.py:10
  10.8 0.8 slice.38
  11.7 0.8 slice.39
  12.6 3.1 %collective-permute-start = (bf16[2,2,64]{2,1,0:T(2,128)(2,1)S(1)}, bf16[2,2,64]{2,1,0:T(2,128)(2,1)S(1)}, u32[]{:S(2)}, u32[]{:S(2)}) collective-permute-start(bf16[2,2,64]{2,1,0:T(2,128)(2,1)S(1)} %pad_maximum_fusion.1), channel_id=1, source_target_pairs={{0,16},{16,32},{32,48},{48,64},{64,80},{80,96},{96,112},{112,128},... | collective-permute-start | bytes 1544 | tf_op jit(solution)/shard_map/ppermute | solution.py:10
  15.7 0.9 convert_multiply_fusion
  18.0 0.8 copy.51
  19.2 0.8 pad_add_fusion
  20.9 1.0 fusion.19
  22.0 0.8 reshape.97
  22.8 8.6 %all-to-all-start = ((bf16[16,2,1024]{2,1,0:T(2,128)(2,1)}), bf16[16,2,1024]{2,1,0:T(2,128)(2,1)S(1)}, u32[]{:S(2)}, u32[]{:S(2)}) async-start(bf16[16,2,1024]{2,1,0:T(2,128)(2,1)} %reshape.97), calls=%async_computation | async-start | bytes 131072 | tf_op jit(solution)/shard_map/all_to_all | solution.py:50
  31.4 7.7 %all-to-all-done = bf16[16,2,1024]{2,1,0:T(2,128)(2,1)S(1)} async-done(((bf16[16,2,1024]{2,1,0:T(2,128)(2,1)}), bf16[16,2,1024]{2,1,0:T(2,128)(2,1)S(1)}, u32[]{:S(2)}, u32[]{:S(2)}) %all-to-all-start) | async-done | bytes 65568 | tf_op jit(solution)/shard_map/all_to_all | solution.py:50
  39.5 3.1 %multiply_reduce_fusion.1 = (f32[32]{0:T(128)S(1)}, f32[32,2048]{1,0:T(8,128)S(1)}) fusion(bf16[32,1024]{1,0:T(8,128)(2,1)S(1)} %all_to_all.23, bf16[1024,2048]{1,0:T(8,128)(2,1)} %param.18, bf16[32,2048]{1,0:T(8,128)(2,1)} %param.19), kind=kOutput, calls=%fused_computation.20 | convolution fusion | flops 134610912 | bytes 4653184 | tf_op jit(solution)/shard_map/dot_general | solution.py:51
  43.4 17.8 %all_to_all.29 = bf16[16,8,2048]{2,1,0:T(8,128)(2,1)} all-to-all(bf16[16,8,2048]{2,1,0:T(8,128)(2,1)S(1)} %fusion.6), channel_id=1, replica_groups=mesh['sp'=16,'tp'=16] {'sp'}, dimensions={0} | all-to-all | bytes 1048576 | tf_op jit(solution)/shard_map/all_to_all | solution.py:74
  61.3 49.6 %all-gather.2.cloned.1.call-done = bf16[256,8,2048]{2,1,0:T(8,128)(2,1)} async-done(((bf16[16,8,2048]{2,1,0:T(8,128)(2,1)}), bf16[256,8,2048]{2,1,0:T(8,128)(2,1)}) %all-gather.2.cloned.1.call-update) | async-done | bytes 8388624 | tf_op jit(solution)/shard_map/all_gather | solution.py:73
  111.0 7.2 %fusion.2 = f32[2048,448]{0,1:T(8,128)S(1)} fusion(bf16[256,8,2048]{2,1,0:T(8,128)(2,1)} %all-gather.2.cloned.1.call-done, bf16[1,2048,448]{1,2,0:T(8,128)(2,1)} %param.23), kind=kOutput, calls=%fused_computation.3 | convolution fusion | flops 3758096384 | bytes 13893632 | tf_op jit(solution)/shard_map/dot_general | solution.py:80
  118.2 5.5 %multiply_convert_fusion = bf16[2048,448]{0,1:T(8,128)(2,1)} fusion(f32[2048,448]{0,1:T(8,128)S(1)} %fusion.2, bf16[256,8,2048]{2,1,0:T(8,128)(2,1)S(1)} %copy-done.3, bf16[1,2048,448]{1,2,0:T(8,128)(2,1)S(1)} %copy-done.4), kind=kOutput, calls=%fused_computation.6 | convolution fusion | flops 3763601408 | bytes 15728640 | tf_op jit(solution)/shard_map/dot_general | solution.py:81
  123.7 3.8 %copy.54 = bf16[2048,448]{1,0:T(8,128)(2,1)} copy(bf16[2048,448]{0,1:T(8,128)(2,1)} %multiply_convert_fusion) | data formatting | bytes 3670016 | tf_op jit(solution)/shard_map/convert_element_type | solution.py:82
  127.5 9.2 %convolution_convert_fusion = bf16[256,8,2048]{2,0,1:T(8,128)(2,1)} fusion(bf16[256,8,448]{2,1,0:T(8,128)(2,1)} %bitcast.43, bf16[1,448,2048]{2,1,0:T(8,128)(2,1)S(1)} %copy-done), kind=kOutput, calls=%fused_computation.5 | convolution fusion | flops 3762290688 | bytes 12058624 | tf_op jit(solution)/shard_map/dot_general | solution.py:83
  137.6 68.4 %reduce-scatter.2.cloned.1.call-done = bf16[16,8,2048]{2,0,1:T(8,128)(2,1)} async-done(((bf16[256,8,2048]{2,0,1:T(8,128)(2,1)}), bf16[16,8,2048]{2,0,1:T(8,128)(2,1)}) %reduce-scatter.2.cloned.1.call-update) | async-done | bytes 524304 | tf_op jit(solution)/shard_map/reduce_scatter | solution.py:87
  206.1 2.1 copy.56
  208.2 7.3 %all-to-all-start.2 = ((bf16[16,8,2048]{2,1,0:T(8,128)(2,1)}), bf16[16,8,2048]{2,1,0:T(8,128)(2,1)S(1)}, u32[]{:S(2)}, u32[]{:S(2)}) async-start(bf16[16,8,2048]{2,1,0:T(8,128)(2,1)} %copy.56), calls=%async_computation.3 | async-start | bytes 1048576 | tf_op jit(solution)/shard_map/all_to_all | solution.py:90
  215.7 8.6 %all-to-all-done.2 = bf16[16,8,2048]{2,1,0:T(8,128)(2,1)S(1)} async-done(((bf16[16,8,2048]{2,1,0:T(8,128)(2,1)}), bf16[16,8,2048]{2,1,0:T(8,128)(2,1)S(1)}, u32[]{:S(2)}, u32[]{:S(2)}) %all-to-all-start.2) | async-done | bytes 524320 | tf_op jit(solution)/shard_map/all_to_all | solution.py:90
  225.2 1.7 multiply_reduce_fusion
  (52 shorter events, 7.0 us)
Async XLA Ops:
  6.5 120.9 %copy-start = (bf16[1,448,2048]{2,1,0:T(8,128)(2,1)S(1)}, bf16[1,448,2048]{2,1,0:T(8,128)(2,1)}, u32[]{:S(2)}) copy-start(bf16[1,448,2048]{2,1,0:T(8,128)(2,1)} %param.25) | copy-start | bytes 5505028
  7.4 11.8 %collective-permute-start.1 = (s32[2]{0:T(128)S(1)}, s32[2]{0:T(128)S(1)}, u32[]{:S(2)}, u32[]{:S(2)}) collective-permute-start(s32[2]{0:T(128)S(1)} %slice.43), channel_id=1, source_target_pairs={{0,16},{16,32},{32,48},{48,64},{64,80},{80,96},{96,112},{112,128},... | collective-permute-start | bytes 32 | tf_op jit(solution)/shard_map/ppermute | solution.py:10
  12.6 8.1 %collective-permute-start = (bf16[2,2,64]{2,1,0:T(2,128)(2,1)S(1)}, bf16[2,2,64]{2,1,0:T(2,128)(2,1)S(1)}, u32[]{:S(2)}, u32[]{:S(2)}) collective-permute-start(bf16[2,2,64]{2,1,0:T(2,128)(2,1)S(1)} %pad_maximum_fusion.1), channel_id=1, source_target_pairs={{0,16},{16,32},{32,48},{48,64},{64,80},{80,96},{96,112},{112,128},... | collective-permute-start | bytes 1544 | tf_op jit(solution)/shard_map/ppermute | solution.py:10
  22.8 16.4 %all-to-all-start = ((bf16[16,2,1024]{2,1,0:T(2,128)(2,1)}), bf16[16,2,1024]{2,1,0:T(2,128)(2,1)S(1)}, u32[]{:S(2)}, u32[]{:S(2)}) async-start(bf16[16,2,1024]{2,1,0:T(2,128)(2,1)} %reshape.97), calls=%async_computation | async-start | bytes 131072 | tf_op jit(solution)/shard_map/all_to_all | solution.py:50
  31.3 79.6 %all-gather.2.cloned.1.call-start = ((), (), s32[]{:S(2)}) async-start(), calls=%async_computation.4 | async-start | bytes 8912896 | tf_op jit(solution)/shard_map/all_gather | solution.py:73
  61.3 144.8 %reduce-scatter.2.cloned.1.call-start = ((), (), s32[]{:S(2)}) async-start(), calls=%async_computation.5 | async-start | bytes 8912896 | tf_op jit(solution)/shard_map/reduce_scatter | solution.py:87
  110.9 7.2 %copy-start.3 = (bf16[256,8,2048]{2,1,0:T(8,128)(2,1)S(1)}, bf16[256,8,2048]{2,1,0:T(8,128)(2,1)}, u32[]{:S(2)}) copy-start(bf16[256,8,2048]{2,1,0:T(8,128)(2,1)} %all-gather.2.cloned.1.call-done) | copy-start | bytes 25165828
  111.0 7.2 %copy-start.4 = (bf16[1,2048,448]{1,2,0:T(8,128)(2,1)S(1)}, bf16[1,2048,448]{1,2,0:T(8,128)(2,1)}, u32[]{:S(2)}) copy-start(bf16[1,2048,448]{1,2,0:T(8,128)(2,1)} %param.24) | copy-start | bytes 5505028
  136.7 0.7 copy-start.1
  136.7 78.9 %copy-start.2 = (f32[32,2]{0,1:T(2,128)S(1)}, f32[32,2]{0,1:T(2,128)}, u32[]{:S(2)}) copy-start(f32[32,2]{0,1:T(2,128)} %param.22) | copy-start | bytes 772
  208.2 16.1 %all-to-all-start.2 = ((bf16[16,8,2048]{2,1,0:T(8,128)(2,1)}), bf16[16,8,2048]{2,1,0:T(8,128)(2,1)S(1)}, u32[]{:S(2)}, u32[]{:S(2)}) async-start(bf16[16,8,2048]{2,1,0:T(8,128)(2,1)} %copy.56), calls=%async_computation.3 | async-start | bytes 1048576 | tf_op jit(solution)/shard_map/all_to_all | solution.py:90
Sparse Core Ops, SparseCore 0:
  61.4 49.4 all-gather.1
  136.8 69.2 reduce-scatter.1
where the time goes:
time: 235 us; the launch traced here: 234 us
  waiting for transfers between devices  134 us (57%)
  matrix products  25.4 us (11%)
  starting transfers between devices  22.4 us (10%)
  blocking collectives  17.8 us (8%)
  between operations  13.6 us (6%)
  local copies, waits for them, and re-layouts  13.1 us (6%)
  other arithmetic  7.69 us (3%)
    reduce_scatter x1, waiting for transfers between devices, local(): lax.psum_scatter(partial_value.astype(jnp.bfloat16), 'tp', scatter_dimens...  68.4 us
    all_gather x1, waiting for transfers between devices, local(): lax.all_gather(lax.all_to_all(dispatch, 'sp', split_axis=0, concat_axis=0...  49.6 us
    all_to_all x1, blocking collectives, local(): lax.all_to_all(dispatch, 'sp', split_axis=0, concat_axis=0, tiled=True)  17.8 us
    dot_general x1, matrix products, local(): jnp.dot(activated, w_down[0], preferred_element_type=jnp.float32)  9.19 us
    all_to_all x1, starting transfers between devices, local(): lax.all_to_all(mixed_rows, 'tp', split_axis=0, concat_axis=1, tiled=True)  8.57 us
    all_to_all x1, waiting for transfers between devices, local(): lax.all_to_all(summed, 'sp', split_axis=0, concat_axis=0, tiled=True)  8.56 us
    all_to_all x1, waiting for transfers between devices, local(): lax.all_to_all(mixed_rows, 'tp', split_axis=0, concat_axis=1, tiled=True)  7.73 us
    all_to_all x1, starting transfers between devices, local(): lax.all_to_all(summed, 'sp', split_axis=0, concat_axis=0, tiled=True)  7.27 us
  transfers between devices with their start and end apart: 6, of which 4 were waited for; matrix products, arithmetic and copies ran while one was open for 3% of the time, Pallas kernels for 0%

commit v1 on v0

--- a/solution.py
+++ b/solution.py
@@ -70,12 +70,9 @@
         "js,jd->sd", placement, repeated, preferred_element_type=jnp.float32
     ).astype(jnp.bfloat16)
     dispatch = dispatch.reshape(experts, capacity, model_width)
-    gathered_piece = lax.all_gather(
-        lax.all_to_all(dispatch, "sp", split_axis=0, concat_axis=0, tiled=True),
-        "tp",
-        axis=0,
-        tiled=True,
-    )
+    shard = lax.all_to_all(dispatch, "sp", split_axis=0, concat_axis=0, tiled=True)
+    copies = jnp.concatenate([shard] * lax.axis_size("tp"), axis=0)
+    gathered_piece = lax.all_to_all(copies, "tp", 0, 0, tiled=True)
     flat_rows = gathered_piece.reshape(-1, model_width)
     gate_part = jnp.dot(flat_rows, w_gate[0], preferred_element_type=jnp.float32)
     up_part = jnp.dot(flat_rows, w_up[0], preferred_element_type=jnp.float32)

time: 235 us -> 367 us (1.56)
  blocking collectives: 17.8 us -> 205 us
  waiting for transfers between devices: 134 us -> 81.9 us
    all_to_all x0 -> x1, blocking collectives: none -> 187 us  [local(): gathered_piece = lax.all_to_all(copies, 'tp', 0, 0, tiled=True)]
    all_gather x1 -> x0, waiting for transfers between devices: 49.6 us -> none  [local(): lax.all_gather(lax.all_to_all(dispatch, 'sp', split_axis=0, concat_axis=0...]
  transfers between devices with their start and end apart: 6 -> 5, of which waited for: 4 -> 3; matrix products, arithmetic and copies ran while one was open for 3% -> 2% of each run, Pallas kernels for 0% -> 0%
where the time goes in v1:
time: 367 us
  blocking collectives  205 us (56%)
  waiting for transfers between devices  81.9 us (22%)
  starting transfers between devices  22.4 us (6%)
  matrix products  22.2 us (6%)
  local copies, waits for them, and re-layouts  13.8 us (4%)
  between operations  13.7 us (4%)
  other arithmetic  7.69 us (2%)
    all_to_all x1, blocking collectives, local(): gathered_piece = lax.all_to_all(copies, 'tp', 0, 0, tiled=True)  187 us
    reduce_scatter x1, waiting for transfers between devices, local(): lax.psum_scatter(partial_value.astype(jnp.bfloat16), 'tp', scatter_dimens...  65.6 us
    all_to_all x1, blocking collectives, local(): lax.all_to_all(dispatch, 'sp', split_axis=0, concat_axis=0, tiled=True)  17.7 us
    dot_general x1, matrix products, local(): jnp.dot(activated, w_down[0], preferred_element_type=jnp.float32)  9.09 us
    all_to_all x1, starting transfers between devices, local(): lax.all_to_all(mixed_rows, 'tp', split_axis=0, concat_axis=1, tiled=True)  8.57 us
    all_to_all x1, waiting for transfers between devices, local(): lax.all_to_all(summed, 'sp', split_axis=0, concat_axis=0, tiled=True)  8.56 us
    all_to_all x1, waiting for transfers between devices, local(): lax.all_to_all(mixed_rows, 'tp', split_axis=0, concat_axis=1, tiled=True)  7.73 us
  transfers between devices with their start and end apart: 5, of which 3 were waited for; matrix products, arithmetic and copies ran while one was open for 2% of the time, Pallas kernels for 0%

profile of v1, /device:TPU:2, one launch (start us, length us, event | category | flops | bytes accessed | tf_op | source)
XLA Modules:
  0.0 366.6 jit_solution(16454332578900371784)
XLA Ops:
  6.5 0.9 slice.43
  7.4 3.4 collective-permute-start.1
  10.8 0.8 slice.38
  11.7 0.8 slice.39
  12.6 3.1 collective-permute-start
  15.7 0.9 convert_multiply_fusion
  18.0 0.8 copy.51
  19.2 0.8 pad_add_fusion
  20.9 1.0 fusion.19
  22.0 0.8 reshape.97
  22.8 8.6 %all-to-all-start = ((bf16[16,2,1024]{2,1,0:T(2,128)(2,1)}), bf16[16,2,1024]{2,1,0:T(2,128)(2,1)S(1)}, u32[]{:S(2)}, u32[]{:S(2)}) async-start(bf16[16,2,1024]{2,1,0:T(2,128)(2,1)} %reshape.97), calls=%async_computation | async-start | bytes 131072 | tf_op jit(solution)/shard_map/all_to_all | solution.py:50
  31.4 7.7 %all-to-all-done = bf16[16,2,1024]{2,1,0:T(2,128)(2,1)S(1)} async-done(((bf16[16,2,1024]{2,1,0:T(2,128)(2,1)}), bf16[16,2,1024]{2,1,0:T(2,128)(2,1)S(1)}, u32[]{:S(2)}, u32[]{:S(2)}) %all-to-all-start) | async-done | bytes 65568 | tf_op jit(solution)/shard_map/all_to_all | solution.py:50
  39.5 3.1 multiply_reduce_fusion.1
  43.4 17.7 %all_to_all.34 = bf16[16,8,2048]{2,1,0:T(8,128)(2,1)S(1)} all-to-all(bf16[16,8,2048]{2,1,0:T(8,128)(2,1)S(1)} %fusion.6), channel_id=1, replica_groups=mesh['sp'=16,'tp'=16] {'sp'}, dimensions={0} | all-to-all | bytes 1048576 | tf_op jit(solution)/shard_map/all_to_all | solution.py:73
  62.0 187.3 %all_to_all.35 = bf16[256,8,2048]{2,1,0:T(8,128)(2,1)S(1)} all-to-all(bf16[256,8,2048]{2,1,0:T(8,128)(2,1)S(1)} %constant_dynamic-update-slice_fusion), channel_id=1, replica_groups=mesh['sp'=16,'tp'=16] {'tp'}, dimensions={0} | all-to-all | bytes 16777216 | tf_op jit(solution)/shard_map/all_to_all | solution.py:75
  249.2 4.0 %fusion.2 = f32[2048,448]{0,1:T(8,128)S(1)} fusion(bf16[256,8,2048]{2,1,0:T(8,128)(2,1)S(1)} %all_to_all.35, bf16[1,2048,448]{1,2,0:T(8,128)(2,1)S(1)} %copy-done.3), kind=kOutput, calls=%fused_computation.3 | convolution fusion | flops 3758096384 | bytes 13893632 | tf_op jit(solution)/shard_map/dot_general | solution.py:77
  253.3 5.5 %multiply_convert_fusion = bf16[2048,448]{0,1:T(8,128)(2,1)} fusion(f32[2048,448]{0,1:T(8,128)S(1)} %fusion.2, bf16[256,8,2048]{2,1,0:T(8,128)(2,1)S(1)} %all_to_all.35, bf16[1,2048,448]{1,2,0:T(8,128)(2,1)S(1)} %copy-done.4), kind=kOutput, calls=%fused_computation.6 | convolution fusion | flops 3763601408 | bytes 15728640 | tf_op jit(solution)/shard_map/dot_general | solution.py:78
  258.8 3.8 %copy.54 = bf16[2048,448]{1,0:T(8,128)(2,1)} copy(bf16[2048,448]{0,1:T(8,128)(2,1)} %multiply_convert_fusion) | data formatting | bytes 3670016 | tf_op jit(solution)/shard_map/convert_element_type | solution.py:79
  262.6 9.1 %convolution_convert_fusion = bf16[256,8,2048]{2,0,1:T(8,128)(2,1)} fusion(bf16[256,8,448]{2,1,0:T(8,128)(2,1)} %bitcast.43, bf16[1,448,2048]{2,1,0:T(8,128)(2,1)S(1)} %copy-done), kind=kOutput, calls=%fused_computation.5 | convolution fusion | flops 3762290688 | bytes 12058624 | tf_op jit(solution)/shard_map/dot_general | solution.py:80
  272.6 65.6 %reduce-scatter.2.cloned.1.call-done = bf16[16,8,2048]{2,0,1:T(8,128)(2,1)} async-done(((bf16[256,8,2048]{2,0,1:T(8,128)(2,1)}), bf16[16,8,2048]{2,0,1:T(8,128)(2,1)}) %reduce-scatter.2.cloned.1.call-update) | async-done | bytes 524304 | tf_op jit(solution)/shard_map/reduce_scatter | solution.py:84
  338.2 2.1 copy.56
  340.4 7.3 %all-to-all-start.3 = ((bf16[16,8,2048]{2,1,0:T(8,128)(2,1)}), bf16[16,8,2048]{2,1,0:T(8,128)(2,1)S(1)}, u32[]{:S(2)}, u32[]{:S(2)}) async-start(bf16[16,8,2048]{2,1,0:T(8,128)(2,1)} %copy.56), calls=%async_computation.4 | async-start | bytes 1048576 | tf_op jit(solution)/shard_map/all_to_all | solution.py:87
  347.9 8.6 %all-to-all-done.3 = bf16[16,8,2048]{2,1,0:T(8,128)(2,1)S(1)} async-done(((bf16[16,8,2048]{2,1,0:T(8,128)(2,1)}), bf16[16,8,2048]{2,1,0:T(8,128)(2,1)S(1)}, u32[]{:S(2)}, u32[]{:S(2)}) %all-to-all-start.3) | async-done | bytes 524320 | tf_op jit(solution)/shard_map/all_to_all | solution.py:87
  357.3 1.7 multiply_reduce_fusion
  (66 shorter events, 7.6 us)
Async XLA Ops:
  6.5 256.1 %copy-start = (bf16[1,448,2048]{2,1,0:T(8,128)(2,1)S(1)}, bf16[1,448,2048]{2,1,0:T(8,128)(2,1)}, u32[]{:S(2)}) copy-start(bf16[1,448,2048]{2,1,0:T(8,128)(2,1)} %param.25) | copy-start | bytes 5505028
  7.4 11.8 %collective-permute-start.1 = (s32[2]{0:T(128)S(1)}, s32[2]{0:T(128)S(1)}, u32[]{:S(2)}, u32[]{:S(2)}) collective-permute-start(s32[2]{0:T(128)S(1)} %slice.43), channel_id=1, source_target_pairs={{0,16},{16,32},{32,48},{48,64},{64,80},{80,96},{96,112},{112,128},... | collective-permute-start | bytes 32 | tf_op jit(solution)/shard_map/ppermute | solution.py:10
  12.6 8.1 %collective-permute-start = (bf16[2,2,64]{2,1,0:T(2,128)(2,1)S(1)}, bf16[2,2,64]{2,1,0:T(2,128)(2,1)S(1)}, u32[]{:S(2)}, u32[]{:S(2)}) collective-permute-start(bf16[2,2,64]{2,1,0:T(2,128)(2,1)S(1)} %pad_maximum_fusion.1), channel_id=1, source_target_pairs={{0,16},{16,32},{32,48},{48,64},{64,80},{80,96},{96,112},{112,128},... | collective-permute-start | bytes 1544 | tf_op jit(solution)/shard_map/ppermute | solution.py:10
  22.8 16.4 %all-to-all-start = ((bf16[16,2,1024]{2,1,0:T(2,128)(2,1)}), bf16[16,2,1024]{2,1,0:T(2,128)(2,1)S(1)}, u32[]{:S(2)}, u32[]{:S(2)}) async-start(bf16[16,2,1024]{2,1,0:T(2,128)(2,1)} %reshape.97), calls=%async_computation | async-start | bytes 131072 | tf_op jit(solution)/shard_map/all_to_all | solution.py:50
  31.3 306.9 %reduce-scatter.2.cloned.1.call-start = ((), (), s32[]{:S(2)}) async-start(), calls=%async_computation.5 | async-start | bytes 8912896 | tf_op jit(solution)/shard_map/reduce_scatter | solution.py:84
  62.0 187.3 %copy-start.3 = (bf16[1,2048,448]{1,2,0:T(8,128)(2,1)S(1)}, bf16[1,2048,448]{1,2,0:T(8,128)(2,1)}, u32[]{:S(2)}) copy-start(bf16[1,2048,448]{1,2,0:T(8,128)(2,1)} %param.23) | copy-start | bytes 5505028
  249.2 4.0 %copy-start.4 = (bf16[1,2048,448]{1,2,0:T(8,128)(2,1)S(1)}, bf16[1,2048,448]{1,2,0:T(8,128)(2,1)}, u32[]{:S(2)}) copy-start(bf16[1,2048,448]{1,2,0:T(8,128)(2,1)} %param.24) | copy-start | bytes 5505028
  271.7 0.7 copy-start.1
  271.7 76.1 %copy-start.2 = (f32[32,2]{0,1:T(2,128)S(1)}, f32[32,2]{0,1:T(2,128)}, u32[]{:S(2)}) copy-start(f32[32,2]{0,1:T(2,128)} %param.22) | copy-start | bytes 772
  340.4 16.1 %all-to-all-start.3 = ((bf16[16,8,2048]{2,1,0:T(8,128)(2,1)}), bf16[16,8,2048]{2,1,0:T(8,128)(2,1)S(1)}, u32[]{:S(2)}, u32[]{:S(2)}) async-start(bf16[16,8,2048]{2,1,0:T(8,128)(2,1)} %copy.56), calls=%async_computation.4 | async-start | bytes 1048576 | tf_op jit(solution)/shard_map/all_to_all | solution.py:87
Sparse Core Ops, SparseCore 0:
  271.8 66.3 reduce-scatter.1
